TPU v7x, 32 devices: a whole 2x2x4 slice. The times are simulated.
32 devices in a mesh: kv: 4 (over y, x), tp: 8 (over z, core).
Axes of the slice: x: 2, y: 2, z: 4, core: 2. Of those that a mesh axis runs over, the one named last changes fastest.
Arguments:
- tokens: bfloat16 [256, 4096], P(None, ('kv', 'tp')), may hold values from -10 to 10
- past_state: float32 [256, 32, 64, 128], P('kv', 'tp'), may hold values from -6 to 6
- first_gain: float32 [4096], P('kv'), may hold values from 0.1 to 1.9
- first_gate: bfloat16 [4096, 11264], P('kv', 'tp'), may hold values from -0.09375 to 0.09375
- first_up: bfloat16 [4096, 11264], P('kv', 'tp'), may hold values from -0.09375 to 0.09375
- first_down: bfloat16 [11264, 4096], P('tp', 'kv'), may hold values from -0.078125 to 0.078125
- mix_gain: float32 [4096], P('kv'), may hold values from 0.1 to 1.9
- query_weight: bfloat16 [4096, 2048], P('kv', 'tp'), may hold values from -0.09375 to 0.09375
- key_weight: bfloat16 [4096, 2048], P('kv', 'tp'), may hold values from -0.09375 to 0.09375
- value_weight: bfloat16 [4096, 4096], P('kv', 'tp'), may hold values from -0.09375 to 0.09375
- output_gate_weight: bfloat16 [4096, 4096], P('kv', 'tp'), may hold values from -0.09375 to 0.09375
- head_gain: float32 [4096], P('tp'), may hold values from 0.1 to 1.9
- out_weight: bfloat16 [4096, 4096], P('tp', 'kv'), may hold values from -0.125 to 0.125
- second_gain: float32 [4096], P('kv'), may hold values from 0.1 to 1.9
- second_gate: bfloat16 [4096, 11264], P('kv', 'tp'), may hold values from -0.09375 to 0.09375
- second_up: bfloat16 [4096, 11264], P('kv', 'tp'), may hold values from -0.09375 to 0.09375
- second_down: bfloat16 [11264, 4096], P('tp', 'kv'), may hold values from -0.078125 to 0.078125
Outputs:
- mixed: bfloat16 [256, 4096], P(None, ('kv', 'tp'))
- new_state: float32 [256, 32, 64, 128], P('kv', 'tp')
All inputs are finite; a program needn't handle non-finite values.
Results may differ from a plain program's by a relative error of at most 0.033.
Values may be sent and summed in bfloat16 or wider, within the bound.
A program may use at most 128 MiB of HBM per device.

v0:
```python
import jax
import jax.numpy as jnp
from jax import lax
from jax.sharding import PartitionSpec as P

D = 4096
HEADS = 32
HEAD_K = 64
HEAD_V = 128
POS = 16384
EPS_RMS = 1e-06
EPS_GROUP = 1e-05
ROPE_BASE = 10000.0


def rotate(vectors):
    half_width = vectors.shape[-1] // 2
    frequency = ROPE_BASE ** (-jnp.arange(half_width, dtype=jnp.float32) / half_width)
    angles = POS * frequency
    cosine = jnp.cos(angles)
    sine_part = jnp.sin(angles)
    lower = vectors[..., :half_width]
    upper = vectors[..., half_width:]
    return jnp.concatenate(
        [lower * cosine - upper * sine_part, lower * sine_part + upper * cosine], axis=-1
    )


def activate(gate_sum, up_sum, summed):
    inverse_rms = lax.rsqrt(summed / D + EPS_RMS)[:, None]
    return (jax.nn.silu(gate_sum * inverse_rms) * (up_sum * inverse_rms)).astype(jnp.bfloat16)


def channel_mix(widened, gain, w_gate, w_up, w_down):
    widened_f = widened.astype(jnp.float32)
    scaled = (widened_f * gain).astype(jnp.bfloat16)
    squares = jnp.sum(widened_f * widened_f, axis=1)
    gate_part = jnp.dot(scaled, w_gate, preferred_element_type=jnp.float32)
    up_part = jnp.dot(scaled, w_up, preferred_element_type=jnp.float32)
    gate_sum, up_sum, summed = (
        lax.psum(gate_part.astype(jnp.bfloat16), "kv").astype(jnp.float32),
        lax.psum(up_part.astype(jnp.bfloat16), "kv").astype(jnp.float32),
        lax.psum(squares.astype(jnp.bfloat16), "kv").astype(jnp.float32),
    )
    return 0.5 * jnp.dot(
        activate(gate_sum, up_sum, summed), w_down, preferred_element_type=jnp.float32
    )


def token_mix(
    widened,
    past_state,
    gain,
    query_weight,
    key_weight,
    value_weight,
    output_gate_weight,
    head_gain,
    out_weight,
):
    widened_f = widened.astype(jnp.float32)
    scaled = (widened_f * gain).astype(jnp.bfloat16)
    squares = jnp.sum(widened_f * widened_f, axis=1)
    query_part = jnp.dot(scaled, query_weight, preferred_element_type=jnp.float32)
    key_part = jnp.dot(scaled, key_weight, preferred_element_type=jnp.float32)
    value_part = jnp.dot(scaled, value_weight, preferred_element_type=jnp.float32)
    gate_part = jnp.dot(scaled, output_gate_weight, preferred_element_type=jnp.float32)
    queries, keys_now, values_now, gate_now, summed = (
        lax.psum_scatter(
            query_part.astype(jnp.bfloat16), "kv", scatter_dimension=0, tiled=True
        ).astype(jnp.float32),
        lax.psum_scatter(
            key_part.astype(jnp.bfloat16), "kv", scatter_dimension=0, tiled=True
        ).astype(jnp.float32),
        lax.psum_scatter(
            value_part.astype(jnp.bfloat16), "kv", scatter_dimension=0, tiled=True
        ).astype(jnp.float32),
        lax.psum_scatter(
            gate_part.astype(jnp.bfloat16), "kv", scatter_dimension=0, tiled=True
        ).astype(jnp.float32),
        lax.psum_scatter(
            squares.astype(jnp.bfloat16), "kv", scatter_dimension=0, tiled=True
        ).astype(jnp.float32),
    )
    inverse_rms = lax.rsqrt(summed / D + EPS_RMS)[:, None]
    row_count = past_state.shape[0]
    local_heads = past_state.shape[1]
    queries = rotate((queries * inverse_rms).reshape(row_count, local_heads, HEAD_K)) * HEAD_K ** (
        -0.5
    )
    keys_now = rotate((keys_now * inverse_rms).reshape(row_count, local_heads, HEAD_K))
    values_now = (values_now * inverse_rms).reshape(row_count, local_heads, HEAD_V)
    gate_now = gate_now * inverse_rms
    head_level = (lax.axis_index("tp") * local_heads + jnp.arange(local_heads)).astype(jnp.float32)
    retained = 1.0 - jnp.exp2(-5.0 - 16.0 * head_level / (HEADS - 1))
    new_state = (
        retained[None, :, None, None] * past_state
        + keys_now[:, :, :, None] * values_now[:, :, None, :]
    )
    retrieved = jnp.einsum("bhk,bhkv->bhv", queries, new_state, precision=lax.Precision.HIGHEST)
    head_mean = jnp.mean(retrieved, axis=-1, keepdims=True)
    variance = jnp.mean(jnp.square(retrieved - head_mean), axis=-1, keepdims=True)
    normed = ((retrieved - head_mean) * lax.rsqrt(variance + EPS_GROUP)).reshape(
        row_count, local_heads * HEAD_V
    )
    mixed_heads = (jax.nn.silu(gate_now) * (normed * head_gain)).astype(jnp.bfloat16)
    projected = jnp.dot(
        lax.all_gather(mixed_heads, "kv", axis=0, tiled=True),
        out_weight,
        preferred_element_type=jnp.float32,
    )
    return (projected, new_state)


def shards(
    tokens,
    past_state,
    first_gain,
    first_gate,
    first_up,
    first_down,
    mix_gain,
    query_weight,
    key_weight,
    value_weight,
    output_gate_weight,
    head_gain,
    out_weight,
    second_gain,
    second_gate,
    second_up,
    second_down,
):

    def first_section(widened):
        return (channel_mix(widened, first_gain, first_gate, first_up, first_down), None)

    def middle_section(widened):
        return token_mix(
            widened,
            past_state,
            mix_gain,
            query_weight,
            key_weight,
            value_weight,
            output_gate_weight,
            head_gain,
            out_weight,
        )

    def last_section(widened):
        return (channel_mix(widened, second_gain, second_gate, second_up, second_down), None)

    sections = [first_section, middle_section, last_section]
    own_columns = tokens
    widened = lax.all_gather(tokens, "tp", axis=1, tiled=True)
    state_out = past_state
    for section_index in range(3):
        branch_out, produced = sections[section_index](widened)
        if produced is not None:
            state_out = produced
        own_piece = lax.psum_scatter(
            branch_out.astype(jnp.bfloat16), "tp", scatter_dimension=1, tiled=True
        ).astype(jnp.float32)
        own_columns = (own_columns.astype(jnp.float32) + own_piece).astype(jnp.bfloat16)
        if section_index < 2:
            widened = lax.all_gather(own_columns, "tp", axis=1, tiled=True)
    return (own_columns, state_out)


def solution(mesh):
    in_specs = (
        P(None, ("kv", "tp")),
        P("kv", "tp", None, None),
        P("kv"),
        P("kv", "tp"),
        P("kv", "tp"),
        P("tp", "kv"),
        P("kv"),
        P("kv", "tp"),
        P("kv", "tp"),
        P("kv", "tp"),
        P("kv", "tp"),
        P("tp"),
        P("tp", "kv"),
        P("kv"),
        P("kv", "tp"),
        P("kv", "tp"),
        P("tp", "kv"),
    )
    out_specs = (P(None, ("kv", "tp")), P("kv", "tp", None, None))
    return jax.shard_map(shards, mesh=mesh, in_specs=in_specs, out_specs=out_specs, check_vma=False)
```

profile of v0, /device:TPU:0, one launch (start us, length us, event | category | flops | bytes accessed | tf_op | source)
XLA Modules:
  0.0 409.7 jit_solution(10858656113238108868)
XLA Ops:
  7.2 15.8 %all_gather.12 = bf16[256,1024]{1,0:T(8,128)(2,1)S(1)} all-gather(bf16[256,128]{1,0:T(8,128)(2,1)} %param.17), channel_id=1, replica_groups=mesh['kv'=4,'tp'=8] {'tp'}, dimensions={1}, use_global_device_ids=true | all-gather | bytes 589824 | tf_op jit(solution)/shard_map/all_gather | solution.py:156
  23.0 2.5 convolution_convert_fusion.2
  25.6 1.9 convolution_convert_fusion.3
  27.7 10.1 %psum.43 = bf16[256]{0:T(256)(128)(2,1)S(1)} all-reduce(bf16[256]{0:T(256)(128)(2,1)S(1)} %fusion.3), channel_id=1, replica_groups=mesh['kv'=4,'tp'=8] {'kv'}, use_global_device_ids=true, to_apply=%region_2.0 | all-reduce | flops 256 | bytes 1024 | tf_op jit(solution)/shard_map/psum | solution.py:43
  37.8 48.4 %all-reduce.8.cloned.1.call-done = (bf16[256,1408]{1,0:T(8,128)(2,1)}, bf16[256,1408]{1,0:T(8,128)(2,1)}) async-done(((bf16[256,1408]{1,0:T(8,128)(2,1)}, bf16[256,1408]{1,0:T(8,128)(2,1)}), (bf16[256,1408]{1,0:T(8,128)(2,1)}, bf16[256,1408]{1,0:T(8,128)(2,1)})) %all-reduce.8.cloned.1.call-update) | async-done | bytes 1441808 | tf_op jit(solution)/shard_map/psum | solution.py:42
  86.2 3.5 fusion
  89.7 1.0 copy.24
  90.8 31.2 %reduce-scatter.22.cloned.1.call-done = bf16[128,256]{1,0:T(8,128)(2,1)} async-done(((bf16[1024,256]{1,0:T(8,128)(2,1)}), bf16[128,256]{1,0:T(8,128)(2,1)}) %reduce-scatter.22.cloned.1.call-update) | async-done | bytes 65552
  123.0 14.0 %all_gather.13 = bf16[256,1024]{1,0:T(8,128)(2,1)S(1)} all-gather(bf16[256,128]{1,0:T(8,128)(2,1)S(1)} %add_convert_fusion.2), channel_id=1, replica_groups=mesh['kv'=4,'tp'=8] {'tp'}, dimensions={1}, use_global_device_ids=true | all-gather | bytes 589824 | tf_op jit(solution)/shard_map/all_gather | solution.py:167
  137.1 2.0 convolution_convert_fusion.8
  140.4 2.0 convolution_convert_fusion.7
  142.5 2.4 convolution_convert_fusion.5
  145.1 9.9 %all-reduce = bf16[256]{0:T(256)(128)(2,1)S(1)} all-reduce(bf16[256]{0:T(256)(128)(2,1)S(1)} %fusion.5), channel_id=4, replica_groups=mesh['kv'=4,'tp'=8] {'kv'}, use_global_device_ids=true, to_apply=%region_7.8.clone | all-reduce | flops 256 | bytes 1024
  155.2 2.4 convolution_convert_fusion.6
  157.8 4.2 %reduce-scatter.16.cloned.1.call-done = bf16[64,256]{1,0:T(8,128)(2,1)} async-done(((bf16[256,256]{1,0:T(8,128)(2,1)}), bf16[64,256]{1,0:T(8,128)(2,1)}) %reduce-scatter.16.cloned.1.call-update) | async-done | bytes 32784 | tf_op jit(solution)/shard_map/reduce_scatter | solution.py:69
  162.0 26.8 %reduce-scatter.18.cloned.1.call-done = bf16[64,256]{1,0:T(8,128)(2,1)} async-done(((bf16[256,256]{1,0:T(8,128)(2,1)}), bf16[64,256]{1,0:T(8,128)(2,1)}) %reduce-scatter.18.cloned.1.call-update) | async-done | bytes 32784 | tf_op jit(solution)/shard_map/reduce_scatter | solution.py:72
  190.2 26.1 %reduce-scatter.20.cloned.1.call-done = bf16[64,512]{1,0:T(8,128)(2,1)} async-done(((bf16[256,512]{1,0:T(8,128)(2,1)}), bf16[64,512]{1,0:T(8,128)(2,1)}) %reduce-scatter.20.cloned.1.call-update) | async-done | bytes 65552 | tf_op jit(solution)/shard_map/reduce_scatter | solution.py:75
  217.3 5.3 %multiply_add_fusion = f32[64,4,64,128]{3,2,1,0:T(8,128)S(1)} fusion(f32[64,4,64,128]{3,2,1,0:T(8,128)} %param.18, f32[64,4,128]{2,1,0:T(4,128)S(1)} %mul.290, f32[64,4,64]{2,1,0:T(4,128)S(1)} %copy.21, f32[4]{0:T(128)S(1)} %exponential_subtract_fusion), kind=kLoop, calls=%fused_computation | loop fusion | flops 6291456 | bytes 16973840 | tf_op jit(solution)/shard_map/add | solution.py:97
  222.6 7.3 %fusion.30 = f32[64,4,1,128]{3,2,1,0:T(1,128)S(1)} fusion(f32[64,4,64,1]{2,3,1,0:T(1,128)S(1)} %copy.22, f32[64,4,64,128]{3,2,1,0:T(8,128)S(1)} %multiply_add_fusion), kind=kOutput, calls=%fused_computation.64 | convolution fusion | flops 25165824 | bytes 8585216 | tf_op jit(solution)/shard_map/bhk,bhkv->bhv/dot_general | solution.py:100
  230.6 12.7 %reduce-scatter.14.cloned.1.call-done = bf16[64,512]{1,0:T(8,128)(2,1)} async-done(((bf16[256,512]{1,0:T(8,128)(2,1)}), bf16[64,512]{1,0:T(8,128)(2,1)}) %reduce-scatter.14.cloned.1.call-update) | async-done | bytes 65552 | tf_op jit(solution)/shard_map/reduce_scatter | solution.py:78
  244.3 9.3 %all_gather.14 = bf16[256,512]{1,0:T(8,128)(2,1)S(1)} all-gather(bf16[64,512]{1,0:T(8,128)(2,1)S(1)} %fusion.21), channel_id=1, replica_groups=mesh['kv'=4,'tp'=8] {'kv'}, dimensions={0}, use_global_device_ids=true | all-gather | bytes 327680 | tf_op jit(solution)/shard_map/all_gather | solution.py:108
  253.6 1.7 convolution_convert_fusion.4
  255.2 1.0 copy.26
  256.3 31.4 %reduce-scatter.24.cloned.1.call-done = bf16[128,256]{1,0:T(8,128)(2,1)} async-done(((bf16[1024,256]{1,0:T(8,128)(2,1)}), bf16[128,256]{1,0:T(8,128)(2,1)}) %reduce-scatter.24.cloned.1.call-update) | async-done | bytes 65552
  288.7 14.2 %all_gather.15 = bf16[256,1024]{1,0:T(8,128)(2,1)S(1)} all-gather(bf16[256,128]{1,0:T(8,128)(2,1)S(1)} %add_convert_fusion.1), channel_id=1, replica_groups=mesh['kv'=4,'tp'=8] {'tp'}, dimensions={1}, use_global_device_ids=true | all-gather | bytes 589824 | tf_op jit(solution)/shard_map/all_gather | solution.py:167
  302.8 3.7 convolution_convert_fusion
  306.5 1.9 convolution_convert_fusion.1
  308.6 10.2 %psum.46 = bf16[256]{0:T(256)(128)(2,1)S(1)} all-reduce(bf16[256]{0:T(256)(128)(2,1)S(1)} %fusion.7), channel_id=1, replica_groups=mesh['kv'=4,'tp'=8] {'kv'}, use_global_device_ids=true, to_apply=%region_16.17 | all-reduce | flops 256 | bytes 1024 | tf_op jit(solution)/shard_map/psum | solution.py:43
  318.9 46.7 %all-reduce.6.cloned.1.call-done = (bf16[256,1408]{1,0:T(8,128)(2,1)}, bf16[256,1408]{1,0:T(8,128)(2,1)}) async-done(((bf16[256,1408]{1,0:T(8,128)(2,1)}, bf16[256,1408]{1,0:T(8,128)(2,1)}), (bf16[256,1408]{1,0:T(8,128)(2,1)}, bf16[256,1408]{1,0:T(8,128)(2,1)})) %all-reduce.6.cloned.1.call-update) | async-done | bytes 1441808 | tf_op jit(solution)/shard_map/psum | solution.py:42
  365.6 3.4 fusion.1
  369.0 1.0 copy.28
  370.0 31.6 %reduce-scatter.26.cloned.1.call-done = bf16[128,256]{1,0:T(8,128)(2,1)} async-done(((bf16[1024,256]{1,0:T(8,128)(2,1)}), bf16[128,256]{1,0:T(8,128)(2,1)}) %reduce-scatter.26.cloned.1.call-update) | async-done | bytes 65552
  (69 shorter events, 9.5 us)
Async XLA Ops:
  7.2 15.9 %copy-start = (bf16[1024,1408]{1,0:T(8,128)(2,1)S(1)}, bf16[1024,1408]{1,0:T(8,128)(2,1)}, u32[]{:S(2)}) copy-start(bf16[1024,1408]{1,0:T(8,128)(2,1)} %param.21) | copy-start | bytes 8650756
  7.2 18.4 %copy-start.6 = (f32[1024]{0:T(1024)S(1)}, f32[1024]{0:T(1024)}, u32[]{:S(2)}) copy-start(f32[1024]{0:T(1024)} %param.19) | copy-start | bytes 12292
  7.2 79.0 %all-reduce.8.cloned.1.call-start = ((), (), s32[]{:S(2)}) async-start(), calls=%async_computation.15 | async-start | bytes 2883584 | tf_op jit(solution)/shard_map/psum | solution.py:42
  7.2 18.3 %copy-start.4 = (bf16[1024,1408]{1,0:T(8,128)(2,1)S(1)}, bf16[1024,1408]{1,0:T(8,128)(2,1)}, u32[]{:S(2)}) copy-start(bf16[1024,1408]{1,0:T(8,128)(2,1)} %param.20) | copy-start | bytes 8650756
  27.5 94.6 %reduce-scatter.22.cloned.1.call-start = ((), (), s32[]{:S(2)}) async-start(), calls=%async_computation.11 | async-start | bytes 589824
  86.2 36.8 %copy-start.2 = (bf16[256,128]{1,0:T(8,128)(2,1)S(1)}, bf16[256,128]{1,0:T(8,128)(2,1)}, u32[]{:S(2)}) copy-start(bf16[256,128]{1,0:T(8,128)(2,1)} %param.17) | copy-start | bytes 196612
  86.2 50.9 %copy-start.7 = (f32[1024]{0:T(1024)S(1)}, f32[1024]{0:T(1024)}, u32[]{:S(2)}) copy-start(f32[1024]{0:T(1024)} %param.23) | copy-start | bytes 12292
  89.7 49.5 %copy-start.9 = (u32[32]{0:T(128)S(1)}, u32[32]{0:T(128)}, u32[]{:S(2)}) copy-start(u32[32]{0:T(128)} %constant.53) | copy-start | bytes 388
  90.7 71.3 %reduce-scatter.16.cloned.1.call-start = ((), (), s32[]{:S(2)}) async-start(), calls=%async_computation.8 | async-start | bytes 163840 | tf_op jit(solution)/shard_map/reduce_scatter | solution.py:69
  139.1 49.7 %reduce-scatter.18.cloned.1.call-start = ((), (), s32[]{:S(2)}) async-start(), calls=%async_computation.9 | async-start | bytes 163840 | tf_op jit(solution)/shard_map/reduce_scatter | solution.py:72
  142.4 73.9 %reduce-scatter.20.cloned.1.call-start = ((), (), s32[]{:S(2)}) async-start(), calls=%async_computation.10 | async-start | bytes 327680 | tf_op jit(solution)/shard_map/reduce_scatter | solution.py:75
  144.9 98.4 %reduce-scatter.14.cloned.1.call-start = ((), (), s32[]{:S(2)}) async-start(), calls=%async_computation.7 | async-start | bytes 327680 | tf_op jit(solution)/shard_map/reduce_scatter | solution.py:78
  157.6 130.1 %reduce-scatter.24.cloned.1.call-start = ((), (), s32[]{:S(2)}) async-start(), calls=%async_computation.12 | async-start | bytes 589824
  222.6 7.4 %copy-start.1 = (f32[64,4,64,128]{3,2,1,0:T(8,128)}, f32[64,4,64,128]{3,2,1,0:T(8,128)S(1)}, u32[]{:S(2)}) copy-start(f32[64,4,64,128]{3,2,1,0:T(8,128)S(1)} %multiply_add_fusion) | copy-start | bytes 25165828
  222.6 20.7 %copy-start.3 = (f32[512]{0:T(512)S(1)}, f32[512]{0:T(512)}, u32[]{:S(2)}) copy-start(f32[512]{0:T(512)} %param.28) | copy-start | bytes 6148
  230.0 72.8 %copy-start.8 = (f32[1024]{0:T(1024)S(1)}, f32[1024]{0:T(1024)}, u32[]{:S(2)}) copy-start(f32[1024]{0:T(1024)} %param.30) | copy-start | bytes 12292
  256.2 109.3 %all-reduce.6.cloned.1.call-start = ((), (), s32[]{:S(2)}) async-start(), calls=%async_computation.14 | async-start | bytes 2883584 | tf_op jit(solution)/shard_map/psum | solution.py:42
  288.6 17.9 %copy-start.5 = (bf16[1024,1408]{1,0:T(8,128)(2,1)S(1)}, bf16[1024,1408]{1,0:T(8,128)(2,1)}, u32[]{:S(2)}) copy-start(bf16[1024,1408]{1,0:T(8,128)(2,1)} %param.31) | copy-start | bytes 8650756
  308.4 93.2 %reduce-scatter.26.cloned.1.call-start = ((), (), s32[]{:S(2)}) async-start(), calls=%async_computation.13 | async-start | bytes 589824
Sparse Core Ops, SparseCore 0:
  27.6 58.5 all-reduce.7
  90.8 31.1 reduce-scatter.21
  139.2 22.7 reduce-scatter.15
  164.6 24.1 reduce-scatter.17
  192.0 24.3 reduce-scatter.19
  218.9 24.3 reduce-scatter.13
  256.4 31.2 reduce-scatter.23
  308.5 56.9 all-reduce.5
  370.1 31.3 reduce-scatter.25
where the time goes:
time: 411 us; the launch traced here: 410 us
  waiting for transfers between devices  259 us (63%)
  blocking collectives  83.5 us (20%)
  matrix products  34.6 us (8%)
  between operations  14.8 us (4%)
  other arithmetic  10.2 us (2%)
  local copies, waits for them, and re-layouts  6.92 us (2%)
    psum x2, waiting for transfers between devices, channel_mix(): lax.psum(up_part.astype(jnp.bfloat16), 'kv').astype(jnp.float32)  95.1 us
    unnamed x12, waiting for transfers between devices  94.3 us
    all_gather x2, blocking collectives, shards(): widened = lax.all_gather(own_columns, 'tp', axis=1, tiled=True)  28.2 us
    reduce_scatter x1, waiting for transfers between devices, token_mix(): lax.psum_scatter(key_part.astype(jnp.bfloat16), 'kv', scatter_dimension=0...  26.8 us
    reduce_scatter x1, waiting for transfers between devices, token_mix(): lax.psum_scatter(value_part.astype(jnp.bfloat16), 'kv', scatter_dimension...  26.1 us
    psum x2, blocking collectives, channel_mix(): lax.psum(squares.astype(jnp.bfloat16), 'kv').astype(jnp.float32)  20.3 us
    all_gather x1, blocking collectives, shards(): widened = lax.all_gather(tokens, 'tp', axis=1, tiled=True)  15.8 us
    reduce_scatter x1, waiting for transfers between devices, token_mix(): lax.psum_scatter(gate_part.astype(jnp.bfloat16), 'kv', scatter_dimension=...  12.7 us
  transfers between devices with their start and end apart: 9, of which 9 were waited for; matrix products, arithmetic and copies ran while one was open for 6% of the time, Pallas kernels for 0%

commit v1 on v0

--- a/solution.py
+++ b/solution.py
@@ -164,7 +164,8 @@
         ).astype(jnp.float32)
         own_columns = (own_columns.astype(jnp.float32) + own_piece).astype(jnp.bfloat16)
         if section_index < 2:
-            widened = lax.all_gather(own_columns, "tp", axis=1, tiled=True)
+            sent = jnp.stack([own_columns] * lax.axis_size("tp"))
+            widened = jnp.concatenate(lax.all_to_all(sent, "tp", 0, 0), axis=1)
     return (own_columns, state_out)
 
 

time: 411 us -> 422 us (1.027)
  waiting for transfers between devices: 259 us -> 275 us
  blocking collectives: 83.5 us -> 72.8 us
    all_gather x2 -> x0, blocking collectives: 28.2 us -> none  [shards(): widened = lax.all_gather(own_columns, 'tp', axis=1, tiled=True)]
    reduce_scatter x1, waiting for transfers between devices: 26.8 us -> 4.01 us  [token_mix(): lax.psum_scatter(key_part.astype(jnp.bfloat16), 'kv', scatter_dimension=0...]
    reduce_scatter x1, waiting for transfers between devices: 4.2 us -> 26.8 us  [token_mix(): lax.psum_scatter(query_part.astype(jnp.bfloat16), 'kv', scatter_dimension...]
    all_to_all x0 -> x1, blocking collectives: none -> 17.7 us  [shards(): widened = jnp.concatenate(lax.all_to_all(sent, 'tp', 0, 0), axis=1)]
    all_to_all x0 -> x1, waiting for transfers between devices: none -> 15.1 us  [shards(): widened = jnp.concatenate(lax.all_to_all(sent, 'tp', 0, 0), axis=1)]
  transfers between devices with their start and end apart: 9 -> 10, of which waited for: 9 -> 10; matrix products, arithmetic and copies ran while one was open for 6% -> 6% of each run, Pallas kernels for 0% -> 0%
where the time goes in v1:
time: 422 us; the launch traced here: 421 us
  waiting for transfers between devices  275 us (65%)
  blocking collectives  72.8 us (17%)
  matrix products  35.4 us (8%)
  between operations  14.8 us (4%)
  other arithmetic  10.5 us (2%)
  local copies, waits for them, and re-layouts  8.79 us (2%)
    psum x2, waiting for transfers between devices, channel_mix(): lax.psum(up_part.astype(jnp.bfloat16), 'kv').astype(jnp.float32)  95.6 us
    unnamed x12, waiting for transfers between devices  94.7 us
    reduce_scatter x1, waiting for transfers between devices, token_mix(): lax.psum_scatter(query_part.astype(jnp.bfloat16), 'kv', scatter_dimension...  26.8 us
    reduce_scatter x1, waiting for transfers between devices, token_mix(): lax.psum_scatter(value_part.astype(jnp.bfloat16), 'kv', scatter_dimension...  25.6 us
    psum x2, blocking collectives, channel_mix(): lax.psum(squares.astype(jnp.bfloat16), 'kv').astype(jnp.float32)  20.2 us
    all_to_all x1, blocking collectives, shards(): widened = jnp.concatenate(lax.all_to_all(sent, 'tp', 0, 0), axis=1)  17.7 us
    all_gather x1, blocking collectives, shards(): widened = lax.all_gather(tokens, 'tp', axis=1, tiled=True)  15.8 us
    all_to_all x1, waiting for transfers between devices, shards(): widened = jnp.concatenate(lax.all_to_all(sent, 'tp', 0, 0), axis=1)  15.1 us
  transfers between devices with their start and end apart: 10, of which 10 were waited for; matrix products, arithmetic and copies ran while one was open for 6% of the time, Pallas kernels for 0%

profile of v1, /device:TPU:0, one launch (start us, length us, event | category | flops | bytes accessed | tf_op | source)
XLA Modules:
  0.0 420.9 jit_solution(5804425401381459526)
XLA Ops:
  7.2 15.8 %all_gather.6 = bf16[256,1024]{1,0:T(8,128)(2,1)S(1)} all-gather(bf16[256,128]{1,0:T(8,128)(2,1)} %param.17), channel_id=1, replica_groups=mesh['kv'=4,'tp'=8] {'tp'}, dimensions={1}, use_global_device_ids=true | all-gather | bytes 589824 | tf_op jit(solution)/shard_map/all_gather | solution.py:156
  23.0 2.5 convolution_convert_fusion.2
  25.6 1.9 convolution_convert_fusion.3
  27.7 10.1 %psum.43 = bf16[256]{0:T(256)(128)(2,1)S(1)} all-reduce(bf16[256]{0:T(256)(128)(2,1)S(1)} %fusion.3), channel_id=1, replica_groups=mesh['kv'=4,'tp'=8] {'kv'}, use_global_device_ids=true, to_apply=%region_2.0 | all-reduce | flops 256 | bytes 1024 | tf_op jit(solution)/shard_map/psum | solution.py:43
  37.8 48.4 %all-reduce.8.cloned.1.call-done = (bf16[256,1408]{1,0:T(8,128)(2,1)}, bf16[256,1408]{1,0:T(8,128)(2,1)}) async-done(((bf16[256,1408]{1,0:T(8,128)(2,1)}, bf16[256,1408]{1,0:T(8,128)(2,1)}), (bf16[256,1408]{1,0:T(8,128)(2,1)}, bf16[256,1408]{1,0:T(8,128)(2,1)})) %all-reduce.8.cloned.1.call-update) | async-done | bytes 1441808 | tf_op jit(solution)/shard_map/psum | solution.py:42
  86.2 3.5 fusion
  89.7 1.0 copy.30
  90.7 31.6 %reduce-scatter.22.cloned.1.call-done = bf16[128,256]{1,0:T(8,128)(2,1)} async-done(((bf16[1024,256]{1,0:T(8,128)(2,1)}), bf16[128,256]{1,0:T(8,128)(2,1)}) %reduce-scatter.22.cloned.1.call-update) | async-done | bytes 65552
  124.2 3.5 all-to-all-start
  127.8 15.1 %all-to-all-done = bf16[8,256,128]{1,2,0:T(8,128)(2,1)S(1)} async-done(((bf16[8,256,128]{1,2,0:T(8,128)(2,1)}), bf16[8,256,128]{1,2,0:T(8,128)(2,1)S(1)}, u32[]{:S(2)}, u32[]{:S(2)}) %all-to-all-start) | async-done | bytes 524320 | tf_op jit(solution)/shard_map/all_to_all | solution.py:168
  144.0 2.0 convolution_convert_fusion.7
  147.4 2.2 convolution_convert_fusion.8
  149.6 2.5 convolution_convert_fusion.5
  152.4 9.8 %all-reduce = bf16[256]{0:T(256)(128)(2,1)S(1)} all-reduce(bf16[256]{0:T(256)(128)(2,1)S(1)} %multiply_reduce_fusion.1), channel_id=4, replica_groups=mesh['kv'=4,'tp'=8] {'kv'}, use_global_device_ids=true, to_apply=%region_7.8.clone | all-reduce | flops 256 | bytes 1024
  162.3 2.6 convolution_convert_fusion.6
  165.1 4.0 reduce-scatter.18.cloned.1.call-done
  169.1 26.8 %reduce-scatter.16.cloned.1.call-done = bf16[64,256]{1,0:T(8,128)(2,1)} async-done(((bf16[256,256]{1,0:T(8,128)(2,1)}), bf16[64,256]{1,0:T(8,128)(2,1)}) %reduce-scatter.16.cloned.1.call-update) | async-done | bytes 32784 | tf_op jit(solution)/shard_map/reduce_scatter | solution.py:69
  197.3 25.6 %reduce-scatter.20.cloned.1.call-done = bf16[64,512]{1,0:T(8,128)(2,1)} async-done(((bf16[256,512]{1,0:T(8,128)(2,1)}), bf16[64,512]{1,0:T(8,128)(2,1)}) %reduce-scatter.20.cloned.1.call-update) | async-done | bytes 65552 | tf_op jit(solution)/shard_map/reduce_scatter | solution.py:75
  223.8 5.3 %multiply_add_fusion = f32[64,4,64,128]{3,2,1,0:T(8,128)S(1)} fusion(f32[64,4,64,128]{3,2,1,0:T(8,128)} %param.18, f32[64,4,128]{2,1,0:T(4,128)S(1)} %mul.294, f32[64,4,64]{2,1,0:T(4,128)S(1)} %copy.26, f32[4]{0:T(128)S(1)} %exponential_subtract_fusion), kind=kLoop, calls=%fused_computation | loop fusion | flops 6291456 | bytes 16973840 | tf_op jit(solution)/shard_map/add | solution.py:97
  229.2 7.3 %fusion.22 = f32[64,4,1,128]{3,2,1,0:T(1,128)S(1)} fusion(f32[64,4,64,1]{2,3,1,0:T(1,128)S(1)} %copy.28, f32[64,4,64,128]{3,2,1,0:T(8,128)S(1)} %multiply_add_fusion), kind=kOutput, calls=%fused_computation.62 | convolution fusion | flops 25165824 | bytes 8585216 | tf_op jit(solution)/shard_map/bhk,bhkv->bhv/dot_general | solution.py:100
  237.1 12.7 %reduce-scatter.14.cloned.1.call-done = bf16[64,512]{1,0:T(8,128)(2,1)} async-done(((bf16[256,512]{1,0:T(8,128)(2,1)}), bf16[64,512]{1,0:T(8,128)(2,1)}) %reduce-scatter.14.cloned.1.call-update) | async-done | bytes 65552 | tf_op jit(solution)/shard_map/reduce_scatter | solution.py:78
  250.8 9.3 %all_gather.7 = bf16[256,512]{1,0:T(8,128)(2,1)S(1)} all-gather(bf16[64,512]{1,0:T(8,128)(2,1)S(1)} %fusion.13), channel_id=1, replica_groups=mesh['kv'=4,'tp'=8] {'kv'}, dimensions={0}, use_global_device_ids=true | all-gather | bytes 327680 | tf_op jit(solution)/shard_map/all_gather | solution.py:108
  260.1 1.7 convolution_convert_fusion.4
  261.7 1.0 copy.32
  262.8 31.4 %reduce-scatter.24.cloned.1.call-done = bf16[128,256]{1,0:T(8,128)(2,1)} async-done(((bf16[1024,256]{1,0:T(8,128)(2,1)}), bf16[128,256]{1,0:T(8,128)(2,1)}) %reduce-scatter.24.cloned.1.call-update) | async-done | bytes 65552
  295.4 17.7 %all_to_all.10 = bf16[8,256,128]{1,2,0:T(8,128)(2,1)S(1)} all-to-all(bf16[8,256,128]{1,2,0:T(8,128)(2,1)S(1)} %stack.5), channel_id=1, replica_groups=mesh['kv'=4,'tp'=8] {'tp'}, dimensions={0} | all-to-all | bytes 1048576 | tf_op jit(solution)/shard_map/all_to_all | solution.py:168
  313.3 3.9 convolution_convert_fusion
  317.2 1.9 convolution_convert_fusion.1
  319.3 10.1 %psum.46 = bf16[256]{0:T(256)(128)(2,1)S(1)} all-reduce(bf16[256]{0:T(256)(128)(2,1)S(1)} %multiply_reduce_fusion), channel_id=1, replica_groups=mesh['kv'=4,'tp'=8] {'kv'}, use_global_device_ids=true, to_apply=%region_16.17 | all-reduce | flops 256 | bytes 1024 | tf_op jit(solution)/shard_map/psum | solution.py:43
  329.5 47.2 %all-reduce.6.cloned.1.call-done = (bf16[256,1408]{1,0:T(8,128)(2,1)}, bf16[256,1408]{1,0:T(8,128)(2,1)}) async-done(((bf16[256,1408]{1,0:T(8,128)(2,1)}, bf16[256,1408]{1,0:T(8,128)(2,1)}), (bf16[256,1408]{1,0:T(8,128)(2,1)}, bf16[256,1408]{1,0:T(8,128)(2,1)})) %all-reduce.6.cloned.1.call-update) | async-done | bytes 1441808 | tf_op jit(solution)/shard_map/psum | solution.py:42
  376.7 3.4 fusion.1
  381.2 31.6 %reduce-scatter.26.cloned.1.call-done = bf16[128,256]{1,0:T(8,128)(2,1)} async-done(((bf16[1024,256]{1,0:T(8,128)(2,1)}), bf16[128,256]{1,0:T(8,128)(2,1)}) %reduce-scatter.26.cloned.1.call-update) | async-done | bytes 65552
  (78 shorter events, 12.7 us)
Async XLA Ops:
  7.2 15.9 %copy-start = (bf16[1024,1408]{1,0:T(8,128)(2,1)S(1)}, bf16[1024,1408]{1,0:T(8,128)(2,1)}, u32[]{:S(2)}) copy-start(bf16[1024,1408]{1,0:T(8,128)(2,1)} %param.21) | copy-start | bytes 8650756
  7.2 18.4 %copy-start.9 = (f32[1024]{0:T(1024)S(1)}, f32[1024]{0:T(1024)}, u32[]{:S(2)}) copy-start(f32[1024]{0:T(1024)} %param.19) | copy-start | bytes 12292
  7.2 79.0 %all-reduce.8.cloned.1.call-start = ((), (), s32[]{:S(2)}) async-start(), calls=%async_computation.17 | async-start | bytes 2883584 | tf_op jit(solution)/shard_map/psum | solution.py:42
  7.2 18.3 %copy-start.7 = (bf16[1024,1408]{1,0:T(8,128)(2,1)S(1)}, bf16[1024,1408]{1,0:T(8,128)(2,1)}, u32[]{:S(2)}) copy-start(bf16[1024,1408]{1,0:T(8,128)(2,1)} %param.20) | copy-start | bytes 8650756
  27.5 94.8 %reduce-scatter.22.cloned.1.call-start = ((), (), s32[]{:S(2)}) async-start(), calls=%async_computation.13 | async-start | bytes 589824
  86.2 37.0 %copy-start.3 = (bf16[256,128]{1,0:T(8,128)(2,1)S(1)}, bf16[256,128]{1,0:T(8,128)(2,1)}, u32[]{:S(2)}) copy-start(bf16[256,128]{1,0:T(8,128)(2,1)} %param.17) | copy-start | bytes 196612
  89.7 53.3 %copy-start.4 = (f32[1024]{0:T(1024)S(1)}, f32[1024]{0:T(1024)}, u32[]{:S(2)}) copy-start(f32[1024]{0:T(1024)} %param.23) | copy-start | bytes 12292
  89.7 56.4 %copy-start.10 = (u32[32]{0:T(128)S(1)}, u32[32]{0:T(128)}, u32[]{:S(2)}) copy-start(u32[32]{0:T(128)} %constant.53) | copy-start | bytes 388
  124.2 18.8 %all-to-all-start = ((bf16[8,256,128]{1,2,0:T(8,128)(2,1)}), bf16[8,256,128]{1,2,0:T(8,128)(2,1)S(1)}, u32[]{:S(2)}, u32[]{:S(2)}) async-start(bf16[8,256,128]{1,2,0:T(8,128)(2,1)} %stack.4), calls=%async_computation | async-start | bytes 1048576 | tf_op jit(solution)/shard_map/all_to_all | solution.py:168
  127.7 41.4 %reduce-scatter.18.cloned.1.call-start = ((), (), s32[]{:S(2)}) async-start(), calls=%async_computation.11 | async-start | bytes 163840 | tf_op jit(solution)/shard_map/reduce_scatter | solution.py:72
  143.2 0.8 copy-start.2
  146.0 49.8 %reduce-scatter.16.cloned.1.call-start = ((), (), s32[]{:S(2)}) async-start(), calls=%async_computation.10 | async-start | bytes 163840 | tf_op jit(solution)/shard_map/reduce_scatter | solution.py:69
  149.6 73.3 %reduce-scatter.20.cloned.1.call-start = ((), (), s32[]{:S(2)}) async-start(), calls=%async_computation.12 | async-start | bytes 327680 | tf_op jit(solution)/shard_map/reduce_scatter | solution.py:75
  152.2 97.7 %reduce-scatter.14.cloned.1.call-start = ((), (), s32[]{:S(2)}) async-start(), calls=%async_computation.9 | async-start | bytes 327680 | tf_op jit(solution)/shard_map/reduce_scatter | solution.py:78
  164.8 129.4 %reduce-scatter.24.cloned.1.call-start = ((), (), s32[]{:S(2)}) async-start(), calls=%async_computation.14 | async-start | bytes 589824
  229.2 7.4 %copy-start.1 = (f32[64,4,64,128]{3,2,1,0:T(8,128)}, f32[64,4,64,128]{3,2,1,0:T(8,128)S(1)}, u32[]{:S(2)}) copy-start(f32[64,4,64,128]{3,2,1,0:T(8,128)S(1)} %multiply_add_fusion) | copy-start | bytes 25165828
  229.2 20.7 %copy-start.6 = (f32[512]{0:T(512)S(1)}, f32[512]{0:T(512)}, u32[]{:S(2)}) copy-start(f32[512]{0:T(512)} %param.28) | copy-start | bytes 6148
  250.8 62.3 %copy-start.5 = (f32[1024]{0:T(1024)S(1)}, f32[1024]{0:T(1024)}, u32[]{:S(2)}) copy-start(f32[1024]{0:T(1024)} %param.30) | copy-start | bytes 12292
  262.8 113.9 %all-reduce.6.cloned.1.call-start = ((), (), s32[]{:S(2)}) async-start(), calls=%async_computation.16 | async-start | bytes 2883584 | tf_op jit(solution)/shard_map/psum | solution.py:42
  313.1 4.1 copy-start.8
  319.1 93.7 %reduce-scatter.26.cloned.1.call-start = ((), (), s32[]{:S(2)}) async-start(), calls=%async_computation.15 | async-start | bytes 589824
Sparse Core Ops, SparseCore 0:
  27.6 58.5 all-reduce.7
  90.8 31.3 reduce-scatter.21
  146.2 22.8 reduce-scatter.17
  171.7 24.1 reduce-scatter.15
  198.5 24.3 reduce-scatter.19
  225.5 24.3 reduce-scatter.13
  262.9 31.2 reduce-scatter.23
  319.2 57.4 all-reduce.5
  381.3 31.4 reduce-scatter.25
